TPU v7x, 512 devices: a whole 4x4x16 slice. The times are simulated.
512 devices in a mesh: ep: 32 (over z, core), tp: 16 (over y, x).
Axes of the slice: x: 4, y: 4, z: 16, core: 2. Of those that a mesh axis runs over, the one named last changes fastest.
Arguments:
- queries: bfloat16 [8192, 2048], P('ep', 'tp'), may hold values from -6 to 6
- key_rows: bfloat16 [8192, 1024], P('ep', 'tp'), may hold values from -6 to 6
- values: bfloat16 [8192, 1024], P('ep', 'tp'), may hold values from -140 to 140
- query_gain: float32 [64], replicated, may hold values from 0.55 to 7.5
- key_gain: float32 [64], replicated, may hold values from 0.55 to 7.5
- mix_gain: float32 [2048], replicated, may hold values from 0.1 to 1.9
- out_weight: bfloat16 [2048, 4096], P(None, 'tp'), may hold values from -0.125 to 0.125
- expert_input: bfloat16 [8192, 4096], P('ep', 'tp'), may hold values from -140 to 140
- expert_gain: float32 [4096], replicated, may hold values from 0.1 to 1.9
- route_ids: int32 [8192, 2], P('ep'), may hold values from 0 to 31, as said below
- route_weights: float32 [8192, 2], P('ep'), may hold values from 0.3 to 1.7
- expert_gate: bfloat16 [32, 4096, 2048], P('ep', None, 'tp'), may hold values from -0.09375 to 0.09375
- expert_up: bfloat16 [32, 4096, 2048], P('ep', None, 'tp'), may hold values from -0.09375 to 0.09375
- expert_down: bfloat16 [32, 2048, 4096], P('ep', None, 'tp'), may hold values from -0.125 to 0.125
Outputs:
- attended: bfloat16 [8192, 4096], P('ep', 'tp')
- expert_mix: bfloat16 [8192, 4096], P('ep', 'tp')
Inputs may be any that keep to these rules, and one draw needn't show every extreme that they name: `route_ids`: the 2 experts of a row differ. In every aligned block of 256 rows no expert is named more than 22 times, and one expert, the same for all blocks, is named exactly 22 times in every block.
All inputs are finite; a program needn't handle non-finite values.
Results may differ from a plain program's by a relative error of at most 0.01.
The roundings to bfloat16 on the way count: a program that leaves them out, or rounds other values in their place, can miss the bound.
Values may be sent and summed in bfloat16 or wider, within the bound.
A program may use at most 64 MiB of HBM per device.

v0:
```python
import math
import jax
import jax.numpy as jnp
from jax import lax
from jax.sharding import Mesh
from jax.sharding import PartitionSpec as P

Q_HEADS = 32
KV_HEADS = 16
HEAD = 64
GRID_W = 64
EP = ("ep_0", "ep_1")
EPS = 1e-06
THETA = 10000.0


def in_one_piece(arrays, axis, dim, along):
    widths = [a.shape[along] for a in arrays]
    both = jnp.concatenate(arrays, axis=along)
    filled = lax.all_gather(both, axis, axis=dim, tiled=True)
    return tuple(jnp.split(filled, [sum(widths[:k]) for k in range(1, len(widths))], axis=along))


def split_up(array, dim, length):
    before, after = (array.shape[:dim], array.shape[dim + 1 :])
    return jnp.moveaxis(array.reshape(*before, length, -1, *after), dim, 0)


def joined_along(blocks, dim):
    lengths = list(blocks.shape[1:])
    lengths[dim] *= blocks.shape[0]
    return jnp.moveaxis(blocks, 0, dim).reshape(lengths)


def exchange_in_order(blocks, axes, order):
    inside = blocks.shape[1:]
    filled = blocks.reshape(*(lax.axis_size(a) for a in axes), *inside)
    for k in order:
        filled = lax.all_to_all(filled, axes[k], k, k, tiled=True)
    return filled.reshape(-1, *inside)


def exchange_by_chip(array, groups, order, split_dim, concat_dim):
    length = lax.axis_size(groups[0]) * lax.axis_size(groups[1])
    blocks = split_up(array, split_dim, length)
    return joined_along(exchange_in_order(blocks, groups, order), concat_dim)


def turn_tables(offset, length):
    half_width = HEAD // 2
    inverse = THETA ** (-jnp.arange(0, half_width, 2, dtype=jnp.float32) / half_width)
    positions = offset + jnp.arange(length, dtype=jnp.int32)
    grid_rows = (positions // GRID_W).astype(jnp.float32)
    grid_cols = (positions % GRID_W).astype(jnp.float32)
    angles = jnp.concatenate([grid_rows[:, None] * inverse, grid_cols[:, None] * inverse], axis=-1)
    return (jnp.cos(angles), jnp.sin(angles))


def norm_turn(source, scale_gain, cosine_table, sine_table):
    length = source.shape[0]
    head_rows = source.astype(jnp.float32).reshape(length, -1, HEAD)
    head_rows = (
        head_rows
        * lax.rsqrt(jnp.mean(head_rows * head_rows, axis=-1, keepdims=True) + EPS)
        * scale_gain
    )
    pair_view = head_rows.reshape(length, head_rows.shape[1], HEAD // 2, 2)
    even_part = pair_view[..., 0]
    odd_part = pair_view[..., 1]
    cosine_part = cosine_table[:, None, :]
    sine_part = sine_table[:, None, :]
    turned = jnp.stack(
        [
            even_part * cosine_part - odd_part * sine_part,
            even_part * sine_part + odd_part * cosine_part,
        ],
        axis=-1,
    )
    return turned.reshape(length, -1).astype(jnp.bfloat16)


def shards(
    queries,
    key_rows,
    values,
    query_gain,
    key_gain,
    mix_gain,
    out_weight,
    expert_input,
    expert_gain,
    route_ids,
    route_weights,
    expert_gate,
    expert_up,
    expert_down,
):
    length = queries.shape[0]
    experts_count = lax.axis_size(EP)
    offset = lax.axis_index(EP) * length
    cosine_table, sine_table = turn_tables(offset, length)
    query_turned = norm_turn(queries, query_gain, cosine_table, sine_table)
    key_turned = norm_turn(key_rows, key_gain, cosine_table, sine_table)
    kv_local = key_rows.shape[1] // HEAD
    group_size = Q_HEADS // KV_HEADS
    query_heads = query_turned.reshape(length, kv_local, group_size, HEAD)
    start_state = (
        jnp.full((kv_local, group_size, length), -jnp.inf, jnp.float32),
        jnp.zeros((kv_local, group_size, length), jnp.float32),
        jnp.zeros((length, kv_local, group_size, HEAD), jnp.float32),
    )
    key_piece, value_piece = in_one_piece((key_turned, values), EP, 0, 1)
    piece_rows = key_piece.shape[0]
    step_rows = 1024
    key_blocks = key_piece.reshape(piece_rows // step_rows, step_rows, kv_local, HEAD)
    value_blocks = value_piece.reshape(piece_rows // step_rows, step_rows, kv_local, HEAD)

    def absorb(current, block_pair):
        running_max, running_sum, running_acc = current
        key_block, value_block = block_pair
        scores = jnp.einsum(
            "rhgd,nhd->hgrn", query_heads, key_block, preferred_element_type=jnp.float32
        ) / math.sqrt(HEAD)
        new_max = jnp.maximum(running_max, jnp.max(scores, axis=-1))
        factor = jnp.exp(running_max - new_max)
        raw_weights = jnp.exp(scores - new_max[..., None])
        new_sum = running_sum * factor + jnp.sum(raw_weights, axis=-1)
        rounded = raw_weights.astype(jnp.bfloat16)
        increment = jnp.einsum(
            "hgrn,nhd->rhgd", rounded, value_block, preferred_element_type=jnp.float32
        )
        new_acc = running_acc * jnp.transpose(factor, (2, 0, 1))[..., None] + increment
        return ((new_max, new_sum, new_acc), None)

    result, unused = lax.scan(absorb, start_state, (key_blocks, value_blocks))
    heads_out = (
        (result[2] / jnp.transpose(result[1], (2, 0, 1))[..., None])
        .reshape(length, -1)
        .astype(jnp.bfloat16)
    )
    top_count = route_ids.shape[1]
    copies = route_ids.shape[0] * top_count
    capacity = (4 * copies + 3 * experts_count - 1) // (3 * experts_count)
    slot_total = experts_count * capacity
    flat_ids = route_ids.reshape(copies)
    hit_marks = (flat_ids[:, None] == jnp.arange(experts_count, dtype=jnp.int32)[None, :]).astype(
        jnp.int32
    )
    earlier = jnp.cumsum(hit_marks, axis=0) - hit_marks
    places = jnp.sum(earlier * hit_marks, axis=1)
    slot_index = flat_ids * capacity + places
    slot_rows = (
        jnp.full((slot_total,), route_ids.shape[0], jnp.int32)
        .at[slot_index]
        .set(jnp.arange(copies, dtype=jnp.int32) // top_count)
    )
    width_local = expert_input.shape[1]
    padded = jnp.concatenate([expert_input, jnp.zeros((1, width_local), jnp.bfloat16)], axis=0)
    outgoing = padded[slot_rows].reshape(experts_count, capacity, width_local)
    arrived = exchange_by_chip(outgoing, ("ep_0", "ep_1"), (1, 0), 0, 0).reshape(
        slot_total, width_local
    )
    piece_float = lax.all_gather(arrived, "tp", axis=1, tiled=True).astype(jnp.float32)
    gain_piece = expert_gain
    scaled_piece = (piece_float * gain_piece).astype(jnp.bfloat16)
    gate_rows = expert_gate[0]
    up_rows = expert_up[0]
    gate_sum = jnp.dot(scaled_piece, gate_rows, preferred_element_type=jnp.float32)
    up_sum = jnp.dot(scaled_piece, up_rows, preferred_element_type=jnp.float32)
    square_sum = jnp.sum(piece_float * piece_float, axis=1)
    row_stat = lax.rsqrt(square_sum / expert_gain.shape[0] + EPS)
    gate_value = gate_sum * row_stat[:, None]
    up_value = up_sum * row_stat[:, None]
    hidden = (jax.nn.silu(gate_value) * up_value).astype(jnp.bfloat16)
    width_out = out_weight.shape[1]
    head_piece, hidden_piece = in_one_piece((heads_out, hidden), "tp", 1, 0)
    head_float = head_piece.astype(jnp.float32)
    gain_piece = mix_gain
    mix_in = (head_float * gain_piece).astype(jnp.bfloat16)
    down_rows = expert_down[0]
    mix_sum = jnp.dot(mix_in, out_weight, preferred_element_type=jnp.float32)
    mix_squares = jnp.sum(head_float * head_float, axis=1)
    expert_sum = jnp.dot(hidden_piece, down_rows, preferred_element_type=jnp.float32)
    attended = (mix_sum * lax.rsqrt(mix_squares / mix_gain.shape[0] + EPS)[:, None]).astype(
        jnp.bfloat16
    )
    expert_back = expert_sum.astype(jnp.bfloat16).reshape(experts_count, capacity, width_out)
    returned = lax.all_to_all(expert_back, EP, split_axis=0, concat_axis=0, tiled=True).reshape(
        slot_total, width_out
    )
    picked = returned[slot_index].astype(jnp.float32) * route_weights.reshape(copies)[:, None]
    expert_mix = jnp.sum(picked.reshape(route_ids.shape[0], top_count, width_out), axis=1).astype(
        jnp.bfloat16
    )
    return (attended, expert_mix)


def solution(mesh):
    torus = Mesh(mesh.devices.reshape(16, 2, mesh.shape["tp"]), ("ep_0", "ep_1", "tp"))
    return jax.shard_map(
        shards,
        mesh=torus,
        in_specs=(
            P(EP, "tp"),
            P(EP, "tp"),
            P(EP, "tp"),
            P(),
            P(),
            P(),
            P(None, "tp"),
            P(EP, "tp"),
            P(),
            P(EP, None),
            P(EP, None),
            P(EP, None, "tp"),
            P(EP, None, "tp"),
            P(EP, None, "tp"),
        ),
        out_specs=(P(EP, "tp"), P(EP, "tp")),
        check_vma=False,
    )
```

profile of v0, /device:TPU:1, one launch (start us, length us, event | category | flops | bytes accessed | tf_op | source)
XLA Modules:
  0.0 310.1 jit_solution(1185379400146651329)
XLA Ops:
  7.2 0.9 fusion.50
  8.1 0.8 fusion.51
  9.4 1.4 pad_maximum_fusion.1
  10.8 0.8 copy.42
  11.9 0.7 broadcast_multiply_fusion.2
  12.9 1.2 reduce-window.6
  14.1 0.2 slice_reduce_fusion
  14.3 0.9 concatenate.47
  15.4 2.4 scatter_custom_fusion
  17.9 2.8 gather_fusion
  20.9 10.5 %all_to_all.15 = bf16[16,2,1,22,256]{4,0,3,2,1:T(8,128)(2,1)S(1)} all-to-all(bf16[16,2,1,22,256]{4,0,3,2,1:T(8,128)(2,1)S(1)} %copy.45), channel_id=1, replica_groups=mesh['ep_0'=16,'ep_1'=2,'tp'=16] {'ep_1'}, dimensions={1} | all-to-all | bytes 720896 | tf_op jit(solution)/shard_map/all_to_all | solution.py:39
  31.4 1.1 copy.46
  32.5 9.6 %all-to-all-start.1 = ((bf16[16,2,1,22,256]{4,1,3,2,0:T(2,128)(2,1)}), bf16[16,2,1,22,256]{4,1,3,2,0:T(2,128)(2,1)S(1)}, u32[]{:S(2)}, u32[]{:S(2)}) async-start(bf16[16,2,1,22,256]{4,1,3,2,0:T(2,128)(2,1)} %copy.46), calls=%async_computation.1 | async-start | bytes 720896 | tf_op jit(solution)/shard_map/all_to_all | solution.py:39
  42.8 0.2 subtract_convert_fusion
  43.2 20.0 %all-to-all-done.1 = bf16[16,2,1,22,256]{4,1,3,2,0:T(2,128)(2,1)S(1)} async-done(((bf16[16,2,1,22,256]{4,1,3,2,0:T(2,128)(2,1)}), bf16[16,2,1,22,256]{4,1,3,2,0:T(2,128)(2,1)S(1)}, u32[]{:S(2)}, u32[]{:S(2)}) %all-to-all-start.1) | async-done | bytes 360480 | tf_op jit(solution)/shard_map/all_to_all | solution.py:39
  63.2 0.8 reshape_reshape_reshape.7
  64.0 0.2 all-gather.8.cloned.1.call-start
  64.3 35.3 %all-gather.4.cloned.1.call-done = bf16[8192,128]{0,1:T(8,128)(2,1)} async-done(((bf16[256,128]{0,1:T(8,128)(2,1)}), bf16[8192,128]{0,1:T(8,128)(2,1)}) %all-gather.4.cloned.1.call-update) | async-done | bytes 2097168 | tf_op jit(solution)/shard_map/all_gather | solution.py:20
  99.5 1.7 fusion.70
  101.2 0.6 copy.54
  101.8 1.6 copy.39
  103.4 0.6 copy.55
  104.0 1.5 copy.40
  105.5 25.7 %while.15 = (s32[]{:T(128)}, f32[1,2,256]{2,1,0:T(2,128)S(1)}, f32[1,2,256]{2,1,0:T(2,128)S(1)}, f32[256,1,2,64]{0,3,2,1:T(8,128)S(1)}, bf16[8,1024,1,64]{1,3,2,...) while((s32[]{:T(128)}, f32[1,2,256]{2,1,0:T(2,128)S(1)}, ...), condition=%wide.region_5.6_spmd.clone, body=%wide.region_2.5_spmd.clone.sunk | while | flops 138513408 | bytes 6914169 | solution.py:135
  105.5 1.4 bitcast_reduce_fusion.3
  106.9 0.4 fusion.81
  107.3 1.4 fusion.82
  108.7 1.4 bitcast_reduce_fusion.3
  110.1 0.4 fusion.81
  110.5 1.4 fusion.82
  111.9 1.4 bitcast_reduce_fusion.3
  113.4 0.4 fusion.81
  113.7 1.4 fusion.82
  115.2 1.4 bitcast_reduce_fusion.3
  116.6 0.4 fusion.81
  117.0 1.4 fusion.82
  118.4 1.4 bitcast_reduce_fusion.3
  119.8 0.4 fusion.81
  120.2 1.4 fusion.82
  121.6 1.4 bitcast_reduce_fusion.3
  123.0 0.4 fusion.81
  123.4 1.4 fusion.82
  124.8 1.4 bitcast_reduce_fusion.3
  126.2 0.4 fusion.81
  126.6 1.4 fusion.82
  128.0 1.4 bitcast_reduce_fusion.3
  129.4 0.4 fusion.81
  129.8 1.4 fusion.82
  131.4 42.5 %all-gather.6.cloned.1.call-done = bf16[704,4096]{1,0:T(8,128)(2,1)} async-done(((bf16[704,256]{1,0:T(8,128)(2,1)}), bf16[704,4096]{1,0:T(8,128)(2,1)}) %all-gather.6.cloned.1.call-update) | async-done | bytes 5767184 | tf_op jit(solution)/shard_map/all_gather | solution.py:163
  173.9 4.0 %fusion.19 = f32[704]{0:T(1024)S(1)} fusion(bf16[704,4096]{1,0:T(8,128)(2,1)} %all-gather.6.cloned.1.call-done), kind=kLoop, calls=%fused_computation.32 | loop fusion | flops 8650048 | bytes 5769984 | tf_op jit(solution)/shard_map/reduce_sum | solution.py:170
  177.9 0.3 copy-done.1
  178.2 3.0 fusion.31
  181.2 1.7 fusion.40
  182.9 0.7 pad_maximum_fusion
  183.7 70.5 %all-gather.8.cloned.1.call-done = bf16[960,2048]{1,0:T(8,128)(2,1)} async-done(((bf16[960,128]{1,0:T(8,128)(2,1)}), bf16[960,2048]{1,0:T(8,128)(2,1)}) %all-gather.8.cloned.1.call-update) | async-done | bytes 3932176 | tf_op jit(solution)/shard_map/all_gather | solution.py:20
  254.2 2.7 fusion.28
  256.9 0.8 reshape.435
  257.8 14.4 %all-to-all-start.2 = ((bf16[32,22,256]{2,1,0:T(8,128)(2,1)}), bf16[32,22,256]{2,1,0:T(8,128)(2,1)S(1)}, u32[]{:S(2)}, u32[]{:S(2)}) async-start(bf16[32,22,256]{2,1,0:T(8,128)(2,1)} %reshape.435), calls=%async_computation.2 | async-start | bytes 786432 | tf_op jit(solution)/shard_map/all_to_all | solution.py:188
  272.3 1.5 fusion.27
  273.8 2.3 fusion.43
  276.2 23.7 %all-to-all-done.2 = bf16[32,22,256]{2,1,0:T(8,128)(2,1)S(1)} async-done(((bf16[32,22,256]{2,1,0:T(8,128)(2,1)}), bf16[32,22,256]{2,1,0:T(8,128)(2,1)S(1)}, u32[]{:S(2)}, u32[]{:S(2)}) %all-to-all-start.2) | async-done | bytes 360480 | tf_op jit(solution)/shard_map/all_to_all | solution.py:188
  300.0 2.0 gather_fusion.1
  301.9 0.3 reshape.437
  302.2 1.4 multiply_reduce_fusion
  (90 shorter events, 3.0 us)
Async XLA Ops:
  7.2 247.0 %copy-start = (bf16[1,2048,256]{2,1,0:T(8,128)(2,1)S(1)}, bf16[1,2048,256]{2,1,0:T(8,128)(2,1)}, u32[]{:S(2)}) copy-start(bf16[1,2048,256]{2,1,0:T(8,128)(2,1)} %param.29) | copy-start | bytes 3145732
  7.2 92.3 %all-gather.4.cloned.1.call-start = ((), (), s32[]{:S(2)}) async-start(), calls=%async_computation.3 | async-start | bytes 2162688 | tf_op jit(solution)/shard_map/all_gather | solution.py:20
  17.9 24.3 %copy-start.2 = (bf16[256,128]{1,0:T(8,128)(2,1)S(1)}, bf16[256,128]{1,0:T(8,128)(2,1)}, u32[]{:S(2)}) copy-start(bf16[256,128]{1,0:T(8,128)(2,1)} %param.16) | copy-start | bytes 196612
  17.9 24.5 %copy-start.4 = (f32[64]{0:T(128)S(1)}, f32[64]{0:T(128)}, u32[]{:S(2)}) copy-start(f32[64]{0:T(128)} %param.19) | copy-start | bytes 772
  32.5 30.6 %all-to-all-start.1 = ((bf16[16,2,1,22,256]{4,1,3,2,0:T(2,128)(2,1)}), bf16[16,2,1,22,256]{4,1,3,2,0:T(2,128)(2,1)S(1)}, u32[]{:S(2)}, u32[]{:S(2)}) async-start(bf16[16,2,1,22,256]{4,1,3,2,0:T(2,128)(2,1)} %copy.46), calls=%async_computation.1 | async-start | bytes 720896 | tf_op jit(solution)/shard_map/all_to_all | solution.py:39
  42.1 131.8 %all-gather.6.cloned.1.call-start = ((), (), s32[]{:S(2)}) async-start(), calls=%async_computation.4 | async-start | bytes 6127616 | tf_op jit(solution)/shard_map/all_gather | solution.py:163
  64.0 190.1 %all-gather.8.cloned.1.call-start = ((), (), s32[]{:S(2)}) async-start(), calls=%async_computation.5 | async-start | bytes 4177920 | tf_op jit(solution)/shard_map/all_gather | solution.py:20
  131.2 46.7 %copy-start.7 = (f32[4096]{0:T(1024)S(1)}, f32[4096]{0:T(1024)}, u32[]{:S(2)}) copy-start(f32[4096]{0:T(1024)} %param.24) | copy-start | bytes 49156
  173.9 4.3 %copy-start.1 = (bf16[704,4096]{1,0:T(8,128)(2,1)S(1)}, bf16[704,4096]{1,0:T(8,128)(2,1)}, u32[]{:S(2)}) copy-start(bf16[704,4096]{1,0:T(8,128)(2,1)} %all-gather.6.cloned.1.call-done) | copy-start | bytes 17301508
  178.2 3.0 copy-start.5
  183.7 88.5 %copy-start.3 = (f32[256,2]{0,1:T(2,128)S(1)}, f32[256,2]{0,1:T(2,128)}, u32[]{:S(2)}) copy-start(f32[256,2]{0,1:T(2,128)} %param.26) | copy-start | bytes 6148
  183.7 90.1 %copy-start.6 = (bf16[2048,256]{1,0:T(8,128)(2,1)S(1)}, bf16[2048,256]{1,0:T(8,128)(2,1)}, u32[]{:S(2)}) copy-start(bf16[2048,256]{1,0:T(8,128)(2,1)} %param.22) | copy-start | bytes 3145732
  183.7 90.1 %copy-start.8 = (f32[2048]{0:T(1024)S(1)}, f32[2048]{0:T(1024)}, u32[]{:S(2)}) copy-start(f32[2048]{0:T(1024)} %param.21) | copy-start | bytes 24580
  257.8 42.1 %all-to-all-start.2 = ((bf16[32,22,256]{2,1,0:T(8,128)(2,1)}), bf16[32,22,256]{2,1,0:T(8,128)(2,1)S(1)}, u32[]{:S(2)}, u32[]{:S(2)}) async-start(bf16[32,22,256]{2,1,0:T(8,128)(2,1)} %reshape.435), calls=%async_computation.2 | async-start | bytes 786432 | tf_op jit(solution)/shard_map/all_to_all | solution.py:188
Sparse Core Ops, SparseCore 0:
  10.9 88.5 all-gather.3
  102.5 71.3 all-gather.5
  183.8 70.3 all-gather.7
where the time goes:
time: 311 us; the launch traced here: 310 us
  waiting for transfers between devices  192 us (62%)
  matrix products  31.9 us (10%)
  starting transfers between devices  24.3 us (8%)
  local copies, waits for them, and re-layouts  20.2 us (6%)
  other arithmetic  16.7 us (5%)
  between operations  14.2 us (5%)
  blocking collectives  10.5 us (3%)
    all_gather x2, waiting for transfers between devices, in_one_piece(): filled = lax.all_gather(both, axis, axis=dim, tiled=True)  106 us
    all_gather x1, waiting for transfers between devices, shards(): lax.all_gather(arrived, 'tp', axis=1, tiled=True).astype(jnp.float32)  42.5 us
    all_to_all x1, waiting for transfers between devices, shards(): lax.all_to_all(expert_back, EP, split_axis=0, concat_axis=0, tiled=True)  23.7 us
    all_to_all x1, waiting for transfers between devices, exchange_in_order(): filled = lax.all_to_all(filled, axes[k], k, k, tiled=True)  20 us
    all_to_all x1, starting transfers between devices, shards(): lax.all_to_all(expert_back, EP, split_axis=0, concat_axis=0, tiled=True)  14.4 us
    dot_general x8, matrix products, absorb(): jnp.einsum('hgrn,nhd->rhgd', rounded, value_block, preferred_element_type...  11.1 us
    dot_general x8, matrix products, absorb(): jnp.einsum('rhgd,nhd->hgrn', query_heads, key_block, preferred_element_ty...  11 us
    all_to_all x1, blocking collectives, exchange_in_order(): filled = lax.all_to_all(filled, axes[k], k, k, tiled=True)  10.5 us
  transfers between devices with their start and end apart: 5, of which 5 were waited for; matrix products, arithmetic and copies ran while one was open for 16% of the time, Pallas kernels for 0%

commit v1 on v0

--- a/solution.py
+++ b/solution.py
@@ -4,6 +4,7 @@
 from jax import lax
 from jax.sharding import Mesh
 from jax.sharding import PartitionSpec as P
+from jax.lax import all_to_all, psum
 
 Q_HEADS = 32
 KV_HEADS = 16
@@ -12,6 +13,13 @@
 EP = ("ep_0", "ep_1")
 EPS = 1e-06
 THETA = 10000.0
+
+
+def notes_derive(piece_in, array_axis):
+    d_next = jnp.stack([piece_in for _ in range(psum(1, axis_name="tp"))], axis=0)
+    e_now = all_to_all(d_next, "tp", 0, 0)
+    v_next = jnp.concatenate(e_now, axis=array_axis)
+    return v_next
 
 
 def in_one_piece(arrays, axis, dim, along):
@@ -160,7 +168,7 @@
     arrived = exchange_by_chip(outgoing, ("ep_0", "ep_1"), (1, 0), 0, 0).reshape(
         slot_total, width_local
     )
-    piece_float = lax.all_gather(arrived, "tp", axis=1, tiled=True).astype(jnp.float32)
+    piece_float = notes_derive(arrived, 1).astype(jnp.float32)
     gain_piece = expert_gain
     scaled_piece = (piece_float * gain_piece).astype(jnp.bfloat16)
     gate_rows = expert_gate[0]

time: 311 us -> 295 us (0.949)
  waiting for transfers between devices: 192 us -> 166 us
  starting transfers between devices: 24.3 us -> 29.6 us
  local copies, waits for them, and re-layouts: 20.2 us -> 23.6 us
    all_gather x1 -> x0, waiting for transfers between devices: 42.5 us -> none  [shards(): lax.all_gather(arrived, 'tp', axis=1, tiled=True).astype(jnp.float32)]
    all_to_all x0 -> x1, waiting for transfers between devices: none -> 9.39 us  [notes_derive(): e_now = all_to_all(d_next, 'tp', 0, 0)]
    all_gather x2, waiting for transfers between devices: 106 us -> 113 us  [in_one_piece(): filled = lax.all_gather(both, axis, axis=dim, tiled=True)]
    all_to_all x0 -> x1, starting transfers between devices: none -> 5.37 us  [notes_derive(): e_now = all_to_all(d_next, 'tp', 0, 0)]
  transfers between devices with their start and end apart: 5 -> 5, of which waited for: 5 -> 5; matrix products, arithmetic and copies ran while one was open for 16% -> 17% of each run, Pallas kernels for 0% -> 0%
where the time goes in v1:
time: 295 us; the launch traced here: 294 us
  waiting for transfers between devices  166 us (56%)
  matrix products  30.5 us (10%)
  starting transfers between devices  29.6 us (10%)
  local copies, waits for them, and re-layouts  23.6 us (8%)
  other arithmetic  19.3 us (7%)
  between operations  14.5 us (5%)
  blocking collectives  10.5 us (4%)
    all_gather x2, waiting for transfers between devices, in_one_piece(): filled = lax.all_gather(both, axis, axis=dim, tiled=True)  113 us
    all_to_all x1, waiting for transfers between devices, shards(): lax.all_to_all(expert_back, EP, split_axis=0, concat_axis=0, tiled=True)  23.6 us
    all_to_all x1, waiting for transfers between devices, exchange_in_order(): filled = lax.all_to_all(filled, axes[k], k, k, tiled=True)  19.9 us
    all_to_all x1, starting transfers between devices, shards(): lax.all_to_all(expert_back, EP, split_axis=0, concat_axis=0, tiled=True)  14.4 us
    dot_general x8, matrix products, absorb(): jnp.einsum('hgrn,nhd->rhgd', rounded, value_block, preferred_element_type...  11.1 us
    dot_general x8, matrix products, absorb(): jnp.einsum('rhgd,nhd->hgrn', query_heads, key_block, preferred_element_ty...  11 us
    all_to_all x1, blocking collectives, exchange_in_order(): filled = lax.all_to_all(filled, axes[k], k, k, tiled=True)  10.5 us
    all_to_all x1, starting transfers between devices, exchange_in_order(): filled = lax.all_to_all(filled, axes[k], k, k, tiled=True)  9.57 us
  transfers between devices with their start and end apart: 5, of which 5 were waited for; matrix products, arithmetic and copies ran while one was open for 17% of the time, Pallas kernels for 0%

profile of v1, /device:TPU:1, one launch (start us, length us, event | category | flops | bytes accessed | tf_op | source)
XLA Modules:
  0.0 294.3 jit_solution(8911861369216282384)
XLA Ops:
  7.2 0.9 fusion.37
  8.1 0.8 fusion.38
  9.4 1.4 pad_maximum_fusion.1
  10.8 0.8 copy.42
  11.9 0.7 broadcast_multiply_fusion.2
  12.9 1.2 reduce-window.6
  14.1 0.2 slice_reduce_fusion
  14.3 0.9 concatenate.47
  15.4 2.4 scatter_custom_fusion
  17.9 2.8 gather_fusion
  20.9 10.5 %all_to_all.20 = bf16[16,2,1,22,256]{4,0,3,2,1:T(8,128)(2,1)S(1)} all-to-all(bf16[16,2,1,22,256]{4,0,3,2,1:T(8,128)(2,1)S(1)} %copy.45), channel_id=1, replica_groups=mesh['ep_0'=16,'ep_1'=2,'tp'=16] {'ep_1'}, dimensions={1} | all-to-all | bytes 720896 | tf_op jit(solution)/shard_map/all_to_all | solution.py:47
  31.4 1.1 copy.46
  32.5 9.6 %all-to-all-start.1 = ((bf16[16,2,1,22,256]{4,1,3,2,0:T(2,128)(2,1)}), bf16[16,2,1,22,256]{4,1,3,2,0:T(2,128)(2,1)S(1)}, u32[]{:S(2)}, u32[]{:S(2)}) async-start(bf16[16,2,1,22,256]{4,1,3,2,0:T(2,128)(2,1)} %copy.46), calls=%async_computation.1 | async-start | bytes 720896 | tf_op jit(solution)/shard_map/all_to_all | solution.py:47
  43.1 19.9 %all-to-all-done.1 = bf16[16,2,1,22,256]{4,1,3,2,0:T(2,128)(2,1)S(1)} async-done(((bf16[16,2,1,22,256]{4,1,3,2,0:T(2,128)(2,1)}), bf16[16,2,1,22,256]{4,1,3,2,0:T(2,128)(2,1)S(1)}, u32[]{:S(2)}, u32[]{:S(2)}) %all-to-all-start.1) | async-done | bytes 360480 | tf_op jit(solution)/shard_map/all_to_all | solution.py:47
  63.2 3.1 %stack.17 = bf16[16,704,256]{2,1,0:T(8,128)(2,1)} broadcast(bf16[704,256]{1,0:T(8,128)(2,1)S(1)} %stack_reshape_reshape_reshape.2), dimensions={1,2} | broadcast | bytes 6127616 | tf_op jit(solution)/shard_map/stack | solution.py:19
  66.3 5.4 %all-to-all-start.2 = ((bf16[16,704,256]{2,1,0:T(8,128)(2,1)}), bf16[16,704,256]{2,1,0:T(8,128)(2,1)}, u32[]{:S(2)}, u32[]{:S(2)}) async-start(bf16[16,704,256]{2,1,0:T(8,128)(2,1)} %stack.17), calls=%async_computation.2 | async-start | bytes 11534336 | tf_op jit(solution)/shard_map/all_to_all | solution.py:20
  71.9 27.6 %all-gather.3.cloned.1.call-done = bf16[8192,128]{0,1:T(8,128)(2,1)} async-done(((bf16[256,128]{0,1:T(8,128)(2,1)}), bf16[8192,128]{0,1:T(8,128)(2,1)}) %all-gather.3.cloned.1.call-update) | async-done | bytes 2097168 | tf_op jit(solution)/shard_map/all_gather | solution.py:28
  99.5 1.7 fusion.57
  101.2 0.6 copy.56
  101.8 1.5 copy.39
  103.4 0.6 copy.57
  104.0 1.6 copy.40
  105.6 25.6 %while.15 = (s32[]{:T(128)}, f32[1,2,256]{2,1,0:T(2,128)S(1)}, f32[1,2,256]{2,1,0:T(2,128)S(1)}, f32[256,1,2,64]{0,3,2,1:T(8,128)S(1)}, bf16[8,1024,1,64]{1,3,2,...) while((s32[]{:T(128)}, f32[1,2,256]{2,1,0:T(2,128)S(1)}, ...), condition=%wide.region_5.6_spmd.clone, body=%wide.region_2.5_spmd.clone.sunk | while | flops 138513408 | bytes 6914169 | solution.py:143
  105.6 1.4 bitcast_reduce_fusion.3
  107.0 0.4 fusion.70
  107.4 1.4 fusion.71
  108.8 1.4 bitcast_reduce_fusion.3
  110.2 0.4 fusion.70
  110.6 1.4 fusion.71
  112.0 1.4 bitcast_reduce_fusion.3
  113.4 0.4 fusion.70
  113.8 1.4 fusion.71
  115.2 1.4 bitcast_reduce_fusion.3
  116.6 0.4 fusion.70
  117.0 1.4 fusion.71
  118.4 1.4 bitcast_reduce_fusion.3
  119.8 0.4 fusion.70
  120.2 1.4 fusion.71
  121.6 1.4 bitcast_reduce_fusion.3
  123.0 0.4 fusion.70
  123.4 1.4 fusion.71
  124.8 1.4 bitcast_reduce_fusion.3
  126.2 0.4 fusion.70
  126.6 1.4 fusion.71
  128.0 1.4 bitcast_reduce_fusion.3
  129.4 0.4 fusion.70
  129.8 1.4 fusion.71
  131.4 9.4 %all-to-all-done.2 = bf16[16,704,256]{2,1,0:T(8,128)(2,1)} async-done(((bf16[16,704,256]{2,1,0:T(8,128)(2,1)}), bf16[16,704,256]{2,1,0:T(8,128)(2,1)}, u32[]{:S(2)}, u32[]{:S(2)}) %all-to-all-start.2) | async-done | bytes 5767200 | tf_op jit(solution)/shard_map/all_to_all | solution.py:20
  140.8 6.5 %fusion.19 = (f32[704]{0:T(1024)S(1)}, bf16[16,88,8,256]{3,2,1,0:T(8,128)(2,1)S(1)}) fusion(bf16[16,704,256]{2,1,0:T(8,128)(2,1)} %all-to-all-done.2, f32[16,256]{1,0:T(8,128)S(1)} %mul.302), kind=kLoop, calls=%fused_computation.32 | loop fusion | flops 14417216 | bytes 11553536 | tf_op jit(solution)/shard_map/reduce_sum | solution.py:178
  147.3 0.8 copy.55
  148.1 0.4 copy-done.5
  148.5 1.7 convolution_multiply_fusion.1
  150.2 1.7 fusion.29
  151.9 0.7 pad_maximum_fusion
  152.7 85.4 %all-gather.5.cloned.1.call-done = bf16[960,2048]{1,0:T(8,128)(2,1)} async-done(((bf16[960,128]{1,0:T(8,128)(2,1)}), bf16[960,2048]{1,0:T(8,128)(2,1)}) %all-gather.5.cloned.1.call-update) | async-done | bytes 3932176 | tf_op jit(solution)/shard_map/all_gather | solution.py:28
  238.1 2.7 fusion.25
  240.8 0.8 reshape.450
  241.7 14.4 %all-to-all-start.3 = ((bf16[32,22,256]{2,1,0:T(8,128)(2,1)}), bf16[32,22,256]{2,1,0:T(8,128)(2,1)S(1)}, u32[]{:S(2)}, u32[]{:S(2)}) async-start(bf16[32,22,256]{2,1,0:T(8,128)(2,1)} %reshape.450), calls=%async_computation.3 | async-start | bytes 786432 | tf_op jit(solution)/shard_map/all_to_all | solution.py:196
  256.2 1.5 fusion.24
  257.8 2.3 fusion.30
  260.1 23.6 %all-to-all-done.3 = bf16[32,22,256]{2,1,0:T(8,128)(2,1)S(1)} async-done(((bf16[32,22,256]{2,1,0:T(8,128)(2,1)}), bf16[32,22,256]{2,1,0:T(8,128)(2,1)S(1)}, u32[]{:S(2)}, u32[]{:S(2)}) %all-to-all-start.3) | async-done | bytes 360480 | tf_op jit(solution)/shard_map/all_to_all | solution.py:196
  283.9 2.0 gather_fusion.1
  285.8 0.3 reshape.452
  286.1 1.4 multiply_reduce_fusion
  (92 shorter events, 3.4 us)
Async XLA Ops:
  7.2 230.9 %copy-start = (bf16[1,2048,256]{2,1,0:T(8,128)(2,1)S(1)}, bf16[1,2048,256]{2,1,0:T(8,128)(2,1)}, u32[]{:S(2)}) copy-start(bf16[1,2048,256]{2,1,0:T(8,128)(2,1)} %param.29) | copy-start | bytes 3145732
  7.2 92.3 %all-gather.3.cloned.1.call-start = ((), (), s32[]{:S(2)}) async-start(), calls=%async_computation.4 | async-start | bytes 2162688 | tf_op jit(solution)/shard_map/all_gather | solution.py:28
  17.9 24.3 %copy-start.2 = (f32[4096]{0:T(1024)S(1)}, f32[4096]{0:T(1024)}, u32[]{:S(2)}) copy-start(f32[4096]{0:T(1024)} %param.24) | copy-start | bytes 49156
  17.9 24.3 %copy-start.1 = (bf16[256,128]{1,0:T(8,128)(2,1)S(1)}, bf16[256,128]{1,0:T(8,128)(2,1)}, u32[]{:S(2)}) copy-start(bf16[256,128]{1,0:T(8,128)(2,1)} %param.16) | copy-start | bytes 196612
  17.9 24.5 %copy-start.4 = (f32[64]{0:T(128)S(1)}, f32[64]{0:T(128)}, u32[]{:S(2)}) copy-start(f32[64]{0:T(128)} %param.19) | copy-start | bytes 772
  32.5 30.5 %all-to-all-start.1 = ((bf16[16,2,1,22,256]{4,1,3,2,0:T(2,128)(2,1)}), bf16[16,2,1,22,256]{4,1,3,2,0:T(2,128)(2,1)S(1)}, u32[]{:S(2)}, u32[]{:S(2)}) async-start(bf16[16,2,1,22,256]{4,1,3,2,0:T(2,128)(2,1)} %copy.46), calls=%async_computation.1 | async-start | bytes 720896 | tf_op jit(solution)/shard_map/all_to_all | solution.py:47
  66.3 74.5 %all-to-all-start.2 = ((bf16[16,704,256]{2,1,0:T(8,128)(2,1)}), bf16[16,704,256]{2,1,0:T(8,128)(2,1)}, u32[]{:S(2)}, u32[]{:S(2)}) async-start(bf16[16,704,256]{2,1,0:T(8,128)(2,1)} %stack.17), calls=%async_computation.2 | async-start | bytes 11534336 | tf_op jit(solution)/shard_map/all_to_all | solution.py:20
  71.7 166.4 %all-gather.5.cloned.1.call-start = ((), (), s32[]{:S(2)}) async-start(), calls=%async_computation.5 | async-start | bytes 4177920 | tf_op jit(solution)/shard_map/all_gather | solution.py:28
  147.3 1.2 copy-start.5
  148.5 1.7 copy-start.6
  152.6 103.4 %copy-start.3 = (f32[256,2]{0,1:T(2,128)S(1)}, f32[256,2]{0,1:T(2,128)}, u32[]{:S(2)}) copy-start(f32[256,2]{0,1:T(2,128)} %param.26) | copy-start | bytes 6148
  152.6 105.1 %copy-start.7 = (bf16[2048,256]{1,0:T(8,128)(2,1)S(1)}, bf16[2048,256]{1,0:T(8,128)(2,1)}, u32[]{:S(2)}) copy-start(bf16[2048,256]{1,0:T(8,128)(2,1)} %param.22) | copy-start | bytes 3145732
  152.6 105.1 %copy-start.8 = (f32[2048]{0:T(1024)S(1)}, f32[2048]{0:T(1024)}, u32[]{:S(2)}) copy-start(f32[2048]{0:T(1024)} %param.21) | copy-start | bytes 24580
  241.7 42.1 %all-to-all-start.3 = ((bf16[32,22,256]{2,1,0:T(8,128)(2,1)}), bf16[32,22,256]{2,1,0:T(8,128)(2,1)S(1)}, u32[]{:S(2)}, u32[]{:S(2)}) async-start(bf16[32,22,256]{2,1,0:T(8,128)(2,1)} %reshape.450), calls=%async_computation.3 | async-start | bytes 786432 | tf_op jit(solution)/shard_map/all_to_all | solution.py:196
Sparse Core Ops, SparseCore 0:
  10.9 88.5 all-gather.2
  152.7 85.3 all-gather.4
